TPU v7x, 32 devices: a whole 2x2x4 slice. The times are simulated.
32 devices in a mesh: grp: 2 (over y), sp: 4 (over z), tp: 4 (over x, core).
Axes of the slice: x: 2, y: 2, z: 4, core: 2. Of those that a mesh axis runs over, the one named last changes fastest.
Arguments:
- query_a: bfloat16 [3072, 1024], P(('grp', 'sp'), 'tp'), parts along dimension 0, may hold values from -6 to 6
- key_a: bfloat16 [3072, 1024], P(('grp', 'sp'), 'tp'), parts along dimension 0, may hold values from -6 to 6
- query_b: bfloat16 [3072, 512], P(('grp', 'sp'), 'tp'), parts along dimension 0, may hold values from -6 to 6
- key_b: bfloat16 [3072, 512], P(('grp', 'sp'), 'tp'), parts along dimension 0, may hold values from -6 to 6
- values_a: bfloat16 [3072, 2048], P(('grp', 'sp'), 'tp'), parts along dimension 0, may hold values from -6 to 6
- values_b: bfloat16 [3072, 2048], P(('grp', 'sp'), 'tp'), parts along dimension 0, may hold values from -6 to 6
- outgate_a: bfloat16 [3072, 2048], P(('grp', 'sp'), 'tp'), parts along dimension 0, may hold values from -8 to 8
- outgate_b: bfloat16 [3072, 2048], P(('grp', 'sp'), 'tp'), parts along dimension 0, may hold values from -8 to 8
- input_pre: float32 [2, 8, 3072], P(None, 'tp', ('grp', 'sp')), parts along dimension 2, may hold values from -8 to 110, as said below
- forget_pre: float32 [2, 8, 3072], P(None, 'tp', ('grp', 'sp')), parts along dimension 2, may hold values from -4 to 16
- resid: bfloat16 [3072, 2048], P(('grp', 'sp', 'tp')), parts along dimension 0, may hold values from -6 to 6
- out_proj: bfloat16 [2048, 2, 2048], P(None, None, 'tp'), may hold values from -0.1875 to 0.1875
- norm_gain: float32 [2048], replicated, may hold values from 0.1 to 1.9
- w_gate: bfloat16 [2048, 5120], P('sp', 'tp'), may hold values from -0.125 to 0.125
- w_up: bfloat16 [2048, 5120], P('sp', 'tp'), may hold values from -0.125 to 0.125
- w_down: bfloat16 [2048, 5120], P('sp', 'tp'), may hold values from -0.078125 to 0.078125
Outputs:
- mixed: bfloat16 [3072, 2048], P(('grp', 'sp', 'tp')), parts along dimension 0
There are 2 independent parts, one for each index of `grp`. A program takes and returns all parts, laid end to end along the dimension named above; an argument that names none is the same for every part. Nothing has to cross between parts.
Inputs may be any that keep to these rules, and one draw needn't show every extreme that they name: `input_pre`: pre-activations of the exponential input gate.
All inputs are finite; a program needn't handle non-finite values.
Results may differ from a plain program's by a relative error of at most 0.014.
Values may be sent and summed in bfloat16 or wider, within the bound.
A program may use at most 64 MiB of HBM per device.

v0:
```python
import functools

import jax
import jax.numpy as jnp
from jax import lax
from jax.experimental import pallas as pl
from jax.experimental.pallas import tpu as pltpu
from jax.sharding import PartitionSpec as P

DKA = 128
DKB = 64
DV = 256


EPS = 1e-06
NEG = -1e30


def summarize(key_heads, value_head_rows, input_log, forget_raw):
    cum_forget = jnp.cumsum(jax.nn.log_sigmoid(forget_raw), axis=1)
    offset_log = input_log - cum_forget
    block_sum = cum_forget[:, -1]
    block_max = block_sum + jnp.max(offset_log, axis=1)
    key_decay = jnp.exp(block_sum[:, None] + offset_log - block_max[:, None])
    scaled_keys = (key_heads.astype(jnp.float32) * jnp.transpose(key_decay)[:, :, None]).astype(
        jnp.bfloat16
    )
    block_memory_state = jnp.einsum(
        "eif,eiw->ifw", scaled_keys, value_head_rows, preferred_element_type=jnp.float32
    )
    return (block_memory_state, block_max, block_sum, offset_log)


def head_outputs(
    query_head_rows,
    key_heads,
    value_head_rows,
    outgate,
    offset_log,
    carried_over,
    mstate,
    key_width,
):
    length = query_head_rows.shape[0]
    run_max = jnp.maximum(lax.cummax(offset_log, axis=1), mstate[:, None])
    causal = jnp.arange(length)[:, None] >= jnp.arange(length)[None, :]
    exponent = jnp.where(causal[None], offset_log[:, None, :] - run_max[:, :, None], -jnp.inf)
    scores = jnp.einsum(
        "thk,shk->hts", query_head_rows, key_heads, preferred_element_type=jnp.float32
    )
    scores = scores * key_width ** (-0.5) * jnp.exp(exponent)
    weights_bf = scores.astype(jnp.bfloat16)
    inner_part = jnp.einsum(
        "hts,shv->thv", weights_bf, value_head_rows, preferred_element_type=jnp.float32
    )
    carried_portion = jnp.einsum(
        "pix,ixe->pie",
        query_head_rows,
        carried_over.astype(jnp.bfloat16),
        preferred_element_type=jnp.float32,
    ) * key_width ** (-0.5)
    carried_portion = (
        carried_portion * jnp.transpose(jnp.exp(mstate[:, None] - run_max))[:, :, None]
    )
    numerator = carried_portion + inner_part
    inv_rms = lax.rsqrt(jnp.mean(numerator * numerator, axis=2, keepdims=True) + EPS)
    gated_out = (
        numerator * inv_rms * jax.nn.sigmoid(outgate.astype(jnp.float32).reshape(numerator.shape))
    )
    return gated_out.reshape(length, -1).astype(jnp.bfloat16)


def shifted(value, axis, shift):
    count = lax.axis_size(axis)
    return lax.ppermute(value, axis, [(i, (i + shift) % count) for i in range(count)])


def swapped(value, axis):
    count = lax.axis_size(axis)
    return lax.ppermute(value, axis, [(i, i ^ 1) for i in range(count)])


def side_swapped(value):
    return swapped(value, "grp")


def column_shifted(value, shift):
    count = lax.axis_size("tp")
    return lax.ppermute(value, "tp", [(i, (i + 2 * shift) % count) for i in range(count)])


def split_wide(value):
    high = lax.reduce_precision(value, 8, 7)
    middle = lax.reduce_precision(value - high, 8, 7)
    return jnp.stack([high, middle, value - high - middle]).astype(jnp.bfloat16)


def entering(state_a, state_b, stats):
    count, mine = lax.axis_size("sp"), lax.axis_index("sp")
    heads, depth_a, width = state_a.shape
    depth_b = state_b.shape[1]
    terms = split_wide(stats).transpose(3, 0, 1, 2).reshape(heads, 1, 12)
    terms = jnp.pad(terms, ((0, 0), (0, 15), (0, width - 12)))
    packed = jnp.concatenate(
        [state_a.astype(jnp.bfloat16), state_b.astype(jnp.bfloat16), terms], axis=1
    )
    parts = [
        lax.ppermute(packed, "sp", [(i, i + step) for i in range(count - step)])
        for step in range(1, count)
    ]
    total = jnp.zeros_like(stats[1])
    highest = jnp.full_like(stats[0], NEG)
    logs = []
    for step in range(1, count):
        got = parts[step - 1][:, depth_a + depth_b, :12].astype(jnp.float32)
        stat = jnp.sum(got.reshape(heads, 3, 2, 2), axis=1).transpose(1, 2, 0)
        logs.append(jnp.where(step <= mine, stat[0] + total, NEG))
        total = total + stat[1]
        highest = jnp.maximum(highest, logs[-1])
    carried_a, carried_b = jnp.zeros_like(state_a), jnp.zeros_like(state_b)
    for step in range(1, count):
        weight = jnp.where(step <= mine, jnp.exp(logs[step - 1] - highest), 0.0)[:, :, None, None]
        part = parts[step - 1].astype(jnp.float32)
        carried_a += weight[0] * part[:, :depth_a]
        carried_b += weight[1] * part[:, depth_a : depth_a + depth_b]
    return carried_a, carried_b, highest


def scatter_pair(partial):
    chips = lax.axis_size("tp") // 2
    me = lax.axis_index("tp")
    chip, core = me // 2, me % 2
    parts = partial.reshape(2, chips, 2, -1, partial.shape[-1])
    away = lax.dynamic_index_in_dim(parts, 1 - core, 2, keepdims=False).astype(jnp.bfloat16)
    kept = lax.dynamic_index_in_dim(parts, core, 2, keepdims=False)
    got = swapped(away, "tp")
    totals = []
    for which in (1, 0):
        both = kept[which].astype(jnp.float32) + got[which].astype(jnp.float32)
        total = lax.dynamic_index_in_dim(both, chip, 0, keepdims=False)
        for step in range(1, chips):
            target = lax.rem(chip + step, chips)
            sent = lax.dynamic_index_in_dim(both, target, 0, keepdims=False).astype(jnp.bfloat16)
            total = total + column_shifted(sent, step).astype(jnp.float32)
        totals.append(total)
    return totals[1] + swapped(totals[0].astype(jnp.bfloat16), "sp").astype(jnp.float32)


def scatter_rows(partial):
    chips = lax.axis_size("tp") // 2
    me = lax.axis_index("tp")
    chip, core = me // 2, me % 2
    parts = partial.reshape(chips, 2, -1, partial.shape[-1])
    away = lax.dynamic_index_in_dim(parts, 1 - core, 1, keepdims=False).astype(jnp.bfloat16)
    kept = lax.dynamic_index_in_dim(parts, core, 1, keepdims=False)
    both = kept.astype(jnp.float32) + swapped(away, "tp").astype(jnp.float32)
    total = lax.dynamic_index_in_dim(both, chip, 0, keepdims=False)
    for step in range(1, chips):
        target = lax.rem(chip + step, chips)
        sent = lax.dynamic_index_in_dim(both, target, 0, keepdims=False).astype(jnp.bfloat16)
        total = total + column_shifted(sent, step).astype(jnp.float32)
    return total


def gather_rows(rows):
    chips = lax.axis_size("tp") // 2
    core = lax.axis_index("tp") % 2
    mine = jnp.stack([rows] + [column_shifted(rows, step) for step in range(1, chips)])
    other = swapped(mine, "tp")
    first = jnp.where(core == 0, mine, other)
    second = jnp.where(core == 0, other, mine)
    gathered = jnp.stack([first, second], axis=1)
    return gathered.reshape(-1, rows.shape[-1])


def by_owner(partial):
    chips = lax.axis_size("tp") // 2
    chip = lax.axis_index("tp") // 2
    parts = partial.reshape(chips, -1, partial.shape[-1])
    order = [
        lax.dynamic_index_in_dim(parts, lax.rem(chip - owner + chips, chips), 0)
        for owner in range(chips)
    ]
    return jnp.concatenate(order).reshape(partial.shape)


def local(
    query_a,
    key_a,
    query_b,
    key_b,
    values_a,
    values_b,
    outgate_a,
    outgate_b,
    input_pre,
    forget_pre,
    resid,
    out_proj,
    norm_gain,
    w_gate,
    w_up,
    w_down,
):
    tokens_dev = query_a.shape[0]
    heads_dev = query_a.shape[1] // DKA
    count, place, part = lax.axis_size("sp"), lax.axis_index("sp"), lax.axis_index("grp")
    depth, units = w_gate.shape
    half = units // 2
    side = lax.rem(place, 2)

    def columns(weight, step):
        target_side = lax.rem(place + step, 2)
        return lax.dynamic_slice_in_dim(weight, target_side * half, half, 1)

    lead = jnp.where(part == 0, w_gate, w_up)
    first_sent = columns(lead, 1)
    lead_parts = [None, shifted(first_sent, "sp", 1)]
    key_heads_a = key_a.reshape(tokens_dev, heads_dev, DKA)
    key_heads_b = key_b.reshape(tokens_dev, heads_dev, DKB)
    value_heads_a = values_a.reshape(tokens_dev, heads_dev, DV)
    value_heads_b = values_b.reshape(tokens_dev, heads_dev, DV)
    state_a, max_a, sum_a, offset_a = summarize(
        key_heads_a, value_heads_a, input_pre[0], forget_pre[0]
    )
    state_b, max_b, sum_b, offset_b = summarize(
        key_heads_b, value_heads_b, input_pre[1], forget_pre[1]
    )
    stats = jnp.stack([jnp.stack([max_a, max_b]), jnp.stack([sum_a, sum_b])])
    lead, w_down, state_a, state_b, stats = lax.optimization_barrier(
        (lead, w_down, state_a, state_b, stats)
    )
    carried_a, carried_b, mstate = entering(state_a, state_b, stats)
    for step in range(2, count):
        lead_parts.append(shifted(columns(lead, step), "sp", step))
    down_mine = lax.dynamic_slice_in_dim(w_down, part * (depth // 2), depth // 2, 0)
    down_parts = [None] + [
        shifted(columns(down_mine, step), "sp", step) for step in range(1, count)
    ]
    hidden_a = head_outputs(
        query_a.reshape(tokens_dev, heads_dev, DKA),
        key_heads_a,
        value_heads_a,
        outgate_a,
        offset_a,
        carried_a,
        mstate[0],
        DKA,
    )
    hidden_b = head_outputs(
        query_b.reshape(tokens_dev, heads_dev, DKB),
        key_heads_b,
        value_heads_b,
        outgate_b,
        offset_b,
        carried_b,
        mstate[1],
        DKB,
    )
    hidden = jnp.stack([hidden_a, hidden_b], axis=1).reshape(tokens_dev, -1)
    proj_weight = out_proj.reshape(out_proj.shape[0], -1)
    row_block = hidden
    attn_rows = scatter_rows(
        lax.dot_general(
            row_block, proj_weight, (((1,), (1,)), ((), ())), preferred_element_type=jnp.float32
        )
    )
    resid_sum = resid.astype(jnp.float32) + attn_rows
    normed = (
        resid_sum
        * lax.rsqrt(jnp.mean(resid_sum * resid_sum, axis=1, keepdims=True) + EPS)
        * norm_gain
    )
    normed = normed.astype(jnp.bfloat16)
    pair_normed = swapped(normed, "sp")
    own = lambda weight: lax.dynamic_slice_in_dim(weight, side * half, half, 1)
    own_trail = jnp.where(part == 0, own(w_up), own(w_gate))
    lead_parts[0] = own(lead)
    trail_parts = [own_trail] + [side_swapped(piece) for piece in lead_parts[1:]]
    other_down = lax.dynamic_slice_in_dim(w_down, (1 - part) * (depth // 2), depth // 2, 0)
    down_parts[0] = own(down_mine)
    down_other = [own(other_down)] + [side_swapped(piece) for piece in down_parts[1:]]

    def placed(pieces, offset, blocks):
        whole = jnp.zeros((blocks * depth, half), jnp.bfloat16)
        for step, (first, second) in enumerate(pieces):
            origin = lax.rem(place - step + count, count) * depth
            whole = lax.dynamic_update_slice_in_dim(whole, first, origin + part * offset, 0)
            if second is not None:
                whole = lax.dynamic_update_slice_in_dim(
                    whole, second, origin + (1 - part) * offset, 0
                )
        return whole

    lead_full = placed([(piece, None) for piece in lead_parts], 0, count)
    trail_full = placed([(piece, None) for piece in trail_parts], 0, count)
    down_full = placed(list(zip(down_parts, down_other)), depth // 2, count)
    rows = jnp.concatenate([gather_rows(normed), gather_rows(pair_normed)])
    lead_act = jnp.dot(rows, lead_full, preferred_element_type=jnp.float32)
    trail_act = jnp.dot(rows, trail_full, preferred_element_type=jnp.float32)
    gate_act = jnp.where(part == 0, lead_act, trail_act)
    up_act = jnp.where(part == 0, trail_act, lead_act)
    inner_act = (jax.nn.silu(gate_act) * up_act).astype(jnp.bfloat16)
    partial = lax.dot_general(
        inner_act, down_full, (((1,), (1,)), ((), ())), preferred_element_type=jnp.float32
    ).astype(jnp.bfloat16)
    partial = partial.reshape(2, -1, partial.shape[-1])
    partial = jnp.stack([by_owner(partial[0]), by_owner(partial[1])])
    return (resid_sum + scatter_pair(partial)).astype(jnp.bfloat16)


MESH = pl.DeviceIdType.MESH
NT = (((1,), (1,)), ((), ()))
TN = (((0,), (0,)), ((), ()))
F32 = jnp.float32
BF16 = jnp.bfloat16
SUBS = 2
LAG_B, LAG_C, LAG_D, RING = 2, 5, 8, 8
VMEM_BYTES = 60 * 2**20


def scan_lanes(value, combine, neutral):
    length = value.shape[1]
    lane = lax.broadcasted_iota(jnp.int32, value.shape, 1)
    step = 1
    while step < length:
        moved = jnp.where(lane >= step, pltpu.roll(value, step, 1), neutral)
        value = combine(value, moved)
        step *= 2
    return value


def fused_body(
    sizes,
    query_a,
    key_a,
    query_b,
    key_b,
    values_a,
    values_b,
    outgate_a,
    outgate_b,
    input_pre,
    forget_pre,
    resid,
    out_proj,
    gain,
    w_gate,
    w_up,
    w_down,
    out_ref,
    qa, ka, qb, kb, va, vb, oga, ogb, inp, fgt, res, proj, gn,
    wg, wu, wd,
    cols, offs, bstate, st_out, st_in, stat_out, stat_in, intra, hidden,
    part1, keep1, dsend1, drecv1, xsend1, xrecv1, rsum,
    rows, act, inner, part2, keep2, dsend2, drecv2, xsend2, xrecv2, zsend2, zrecv2,
    lsem, zs, zr, ys, yr, cs, cr, d1s, d1r, x1s, x1r, ags, agr,
    d2s, d2r, x2s, x2r, z2s, z2r,
):
    count, tokens, heads, depth, half, block, chunk1, _ = sizes
    g, s, t = lax.axis_index("grp"), lax.axis_index("sp"), lax.axis_index("tp")
    x, c = lax.div(t, 2), lax.rem(t, 2)
    core_peer = (g, s, t + 1 - 2 * c)
    x_peer = (g, s, t + 2 - 4 * x)
    y_peer = (1 - g, s, t)
    pair = (g, s + 1 - 2 * lax.rem(s, 2), t)
    part_rows = depth // 2
    sub_rows = part_rows // SUBS

    def remote(src, dst, send, recv, device):
        return pltpu.make_async_remote_copy(
            src_ref=src, dst_ref=dst, send_sem=send, recv_sem=recv,
            device_id=device, device_id_type=MESH,
        )

    barrier = pltpu.get_barrier_semaphore()
    for device in (core_peer, x_peer, y_peer):
        pl.semaphore_signal(barrier, inc=1, device_id=device, device_id_type=MESH)
    for place in range(count):
        @pl.when(place != s)
        def _():
            pl.semaphore_signal(barrier, inc=1, device_id=(g, place, t), device_id_type=MESH)

    side = lax.rem(s, 2)
    own_cols = pl.ds(pl.multiple_of(side * half, 128), half)
    own_rows = pl.ds(pl.multiple_of(s * depth, depth), depth)
    loads = [
        (input_pre, inp), (forget_pre, fgt), (key_a, ka), (key_b, kb), (values_a, va),
        (values_b, vb), (query_a, qa), (query_b, qb), (outgate_a, oga), (outgate_b, ogb),
        (out_proj, proj), (resid, res), (gain, gn),
        (w_gate.at[:, own_cols], wg.at[own_rows]),
        (w_up.at[:, own_cols], wu.at[own_rows]),
        (w_down.at[:, own_cols], wd.at[own_rows]),
    ]
    local = [pltpu.make_async_copy(a, b, lsem.at[i]) for i, (a, b) in enumerate(loads)]
    for copy in local:
        copy.start()

    whole_of = (wg, wu) + (wd,) * SUBS
    held_of = (w_gate, w_up) + (w_down,) * SUBS

    def piece_rows(pid, source, which):
        if pid < 2:
            return pl.ds(pl.multiple_of(source * depth + which * part_rows, part_rows), part_rows)
        start = source * depth + which * part_rows + (pid - 2) * sub_rows
        return pl.ds(pl.multiple_of(start, sub_rows), sub_rows)

    def z_copy(pid, dest):
        start = g * part_rows + (0 if pid < 2 else (pid - 2) * sub_rows)
        size = part_rows if pid < 2 else sub_rows
        src = held_of[pid].at[
            pl.ds(pl.multiple_of(start, sub_rows), size), pl.ds((dest % 2) * half, half)
        ]
        return remote(
            src, whole_of[pid].at[piece_rows(pid, s, g)],
            zs.at[pid, dest], zr.at[pid, s], (g, dest, t),
        )

    def y_copy(pid, source, which):
        place = whole_of[pid].at[piece_rows(pid, source, which)]
        return remote(place, place, ys.at[pid, source], yr.at[pid, source], y_peer)

    def arrived_z(pid, source):
        place = whole_of[pid].at[piece_rows(pid, source, g)]
        remote(place, place, zs.at[pid, source], zr.at[pid, source], y_peer).wait_recv()

    def issue(pids, want):
        for pid in pids:
            for dest in list(range(count)):
                @pl.when(jnp.logical_and(dest < s, want(dest)))
                def _():
                    z_copy(pid, dest).start()
            for dest in reversed(range(count)):
                @pl.when(jnp.logical_and(dest > s, want(dest)))
                def _():
                    z_copy(pid, dest).start()

    last = count - 1
    at_end = jnp.logical_or(s == 0, s == last)

    def far(dest):
        return jnp.logical_or(jnp.logical_not(at_end), jnp.abs(dest - s) == last)

    def near(dest):
        return jnp.logical_not(far(dest))

    def source_at(step):
        up_room, down_room = last - s, s
        small = jnp.minimum(up_room, down_room)
        both = jnp.where(step % 2 == 1, s + (step + 1) // 2, s - step // 2)
        beyond = jnp.where(up_room > down_room, s + step - small, s - step + small)
        return jnp.where(step <= 2 * small, both, beyond)

    def forward(pid, step):
        source = source_at(step)
        arrived_z(pid, source)
        y_copy(pid, source, g).start()

    pl.semaphore_wait(barrier, 3 + count - 1)
    issue((0,), lambda dest: dest < s)
    issue((1,), lambda dest: jnp.logical_and(dest < s, far(dest)))
    issue((0,), lambda dest: dest > s)

    for i in range(2):
        local[i].wait()
    quad = lambda ref: jnp.concatenate([ref[0], ref[1], ref[0], ref[1]], axis=0)
    raw_forget, raw_input = quad(fgt), quad(inp)
    log_forget = jnp.minimum(raw_forget, 0.0) - jnp.log1p(jnp.exp(-jnp.abs(raw_forget)))
    cum = scan_lanes(log_forget, lambda a, b: a + b, 0.0)
    offset = raw_input - cum
    run = scan_lanes(offset, jnp.maximum, NEG)
    fsum = cum[:, tokens - 1 : tokens]
    top = run[:, tokens - 1 : tokens]
    bmax = fsum + top
    decay = jnp.exp(offset - top)
    offs[...] = offset
    group = 2 * heads
    cols[...] = jnp.transpose(jnp.concatenate([decay[:group], run[:group]], axis=0))

    for i in range(2, 6):
        local[i].wait()
    head_lane = lax.div(lax.broadcasted_iota(jnp.int32, (tokens, heads * DKB), 1), DKB)
    state_of = []
    for h in range(heads):
        column = cols[:, h : h + 1]
        scaled = (ka[:, h * DKA : (h + 1) * DKA].astype(F32) * column).astype(BF16)
        state = lax.dot_general(
            scaled, va[:, h * DV : (h + 1) * DV], TN, preferred_element_type=F32
        )
        bstate[h * DKA : (h + 1) * DKA, :] = state
        state_of.append((h * DKA, DKA, h))
    base_b = heads * DKA
    for h in range(heads):
        column = cols[:, heads + h : heads + h + 1]
        scaled = (kb[...].astype(F32) * column).astype(BF16)
        state = lax.dot_general(
            scaled, vb[:, h * DV : (h + 1) * DV], TN, preferred_element_type=F32
        )
        bstate[base_b + h * DKB : base_b + (h + 1) * DKB, :] = state[h * DKB : (h + 1) * DKB]
        state_of.append((base_b + h * DKB, DKB, heads + h))

    chain = [
        remote(st_out, st_in, cs.at[0], cr.at[0], (g, jnp.minimum(s + 1, last), t)),
        remote(stat_out, stat_in, cs.at[1], cr.at[1], (g, jnp.minimum(s + 1, last), t)),
    ]

    def combine_and_send():
        before = stat_in[...]
        total = before + fsum
        after = jnp.maximum(total, bmax)
        keep_old = jnp.exp(total - after)
        keep_new = jnp.exp(jnp.broadcast_to(bmax, total.shape) - after)
        stat_out[...] = after
        wide = lambda row: jnp.concatenate([row] * (DV // 128), axis=1)
        for start, size, h in state_of:
            old = wide(keep_old[h : h + 1, :])
            new = wide(keep_new[h : h + 1, :])
            st_out[start : start + size, :] = (
                old * st_in[start : start + size, :].astype(F32)
                + new * bstate[start : start + size, :]
            ).astype(BF16)
        for copy in chain:
            copy.start()

    @pl.when(s == 0)
    def _():
        st_in[...] = jnp.zeros_like(st_in)
        stat_in[...] = jnp.full_like(stat_in, NEG)
        combine_and_send()
        issue((1,), lambda dest: jnp.logical_and(dest > s, far(dest)))

    for i in range(6, 8):
        local[i].wait()
    causal = lax.broadcasted_iota(jnp.int32, (tokens, tokens), 0) >= lax.broadcasted_iota(
        jnp.int32, (tokens, tokens), 1
    )

    def query_of(h):
        if h < heads:
            return qa[:, h * DKA : (h + 1) * DKA]
        return jnp.where(head_lane == h - heads, qb[...], jnp.zeros_like(qb[...]))

    for h in range(group):
        key = ka[:, h * DKA : (h + 1) * DKA] if h < heads else kb[...]
        value_ref, at = (va, h) if h < heads else (vb, h - heads)
        width = DKA if h < heads else DKB
        scores = lax.dot_general(query_of(h), key, NT, preferred_element_type=F32)
        exponent = jnp.where(causal, offs[h : h + 1, :] - cols[:, group + h : group + h + 1], NEG)
        weights = (scores * width ** (-0.5) * jnp.exp(exponent)).astype(BF16)
        intra[h] = jnp.dot(
            weights, value_ref[:, at * DV : (at + 1) * DV], preferred_element_type=F32
        )

    @pl.when(s > 0)
    def _():
        for copy in chain:
            copy.wait_recv()

    @pl.when(jnp.logical_and(s > 0, s < last))
    def _():
        combine_and_send()
        issue((1,), lambda dest: jnp.logical_and(dest > s, far(dest)))

    for i in range(8, 10):
        local[i].wait()
    for h in range(group):
        width = DKA if h < heads else DKB
        gate_ref, at = (oga, h) if h < heads else (ogb, h - heads)
        state = (
            st_in[h * DKA : (h + 1) * DKA, :] if h < heads else st_in[base_b:, :]
        )
        entering_max = stat_in[h : h + 1, 0:1]
        own_max = cols[:, group + h : group + h + 1]
        top_max = jnp.maximum(own_max, entering_max)
        carried = jnp.dot(query_of(h), state, preferred_element_type=F32)
        numer = carried * (width ** (-0.5) * jnp.exp(entering_max - top_max)) + intra[
            h
        ] * jnp.exp(own_max - top_max)
        inv = lax.rsqrt(jnp.mean(numer * numer, axis=1, keepdims=True) + EPS)
        gated = numer * inv * jax.nn.sigmoid(gate_ref[:, at * DV : (at + 1) * DV].astype(F32))
        hidden[:, h * DV : (h + 1) * DV] = gated.astype(BF16)

    forward(0, 1)

    for i in range(10, 13):
        local[i].wait()
    chunks1 = proj.shape[0] // chunk1

    def block_rows(chip, core):
        return pl.ds(pl.multiple_of((2 * chip + core) * block, 8), block)

    def d1(j):
        return remote(dsend1.at[j], drecv1.at[j], d1s.at[j], d1r.at[j], core_peer)

    def x1(j):
        return remote(xsend1.at[j], xrecv1.at[j], x1s.at[j], x1r.at[j], x_peer)

    def attn_step(j, carry):
        @pl.when(j < chunks1)
        def _():
            weight = proj[pl.ds(pl.multiple_of(j * chunk1, chunk1), chunk1)]
            part1[...] = lax.dot_general(
                hidden[...], weight.reshape(chunk1, hidden.shape[1]), NT,
                preferred_element_type=F32,
            )
            for role in range(2):
                chip = x if role == 0 else 1 - x
                dsend1[j, role] = part1[block_rows(chip, 1 - c)].astype(BF16)
                keep1[j, role] = part1[block_rows(chip, c)]
            d1(j).start()

        @pl.when(j >= 1)
        def _():
            k = j - 1
            d1(k).wait_recv()
            xsend1[k] = (keep1[k, 1] + drecv1[k, 1].astype(F32)).astype(BF16)
            x1(k).start()
            keep1[k, 0] = keep1[k, 0] + drecv1[k, 0].astype(F32)

        return carry

    lax.fori_loop(0, chunks1 + 1, attn_step, 0)
    forward(0, 2)
    for j in range(chunks1):
        span = slice(j * chunk1, (j + 1) * chunk1)
        x1(j).wait_recv()
        rsum[:, span] = res[:, span].astype(F32) + keep1[j, 0] + xrecv1[j].astype(F32)
    summed = rsum[...]
    scale = lax.rsqrt(jnp.mean(summed * summed, axis=1, keepdims=True) + EPS)
    mine = block_rows(x, c)
    rows[0, mine] = (summed * scale * gn[...]).astype(BF16)

    def move(kind, src_place, dst_place, chip, core, device):
        return remote(
            rows.at[src_place, block_rows(chip, core)],
            rows.at[dst_place, block_rows(chip, core)],
            ags.at[kind], agr.at[kind], device,
        )

    own_z = move(2, 0, 1, x, c, pair)
    own_x = move(1, 0, 0, x, c, x_peer)
    own_d = move(0, 0, 0, x, c, core_peer)
    own_z.start()
    own_x.start()
    own_d.start()
    issue((1,), near)
    issue(range(2, 2 + SUBS), lambda dest: dest != s)

    def arrived(kind, place, chip, core):
        move(kind, place, place, chip, core, core_peer).wait_recv()

    forward(0, 3)
    arrived(1, 0, 1 - x, c)
    fwd_x = move(3, 0, 0, 1 - x, c, core_peer)
    fwd_x.start()
    forward(1, 1)
    arrived(2, 1, x, c)
    fwd_zx = move(5, 1, 1, x, c, x_peer)
    fwd_zd = move(4, 1, 1, x, c, core_peer)
    fwd_zx.start()
    fwd_zd.start()

    def arrived_y(pid, source):
        y_copy(pid, source, 1 - g).wait_recv()

    for i in range(13, 16):
        local[i].wait()
    for step in range(1, count):
        arrived_y(0, source_at(step))
    arrived(0, 0, x, 1 - c)
    arrived(3, 0, 1 - x, 1 - c)
    act[0] = jnp.dot(rows[0], wg[...], preferred_element_type=F32)
    arrived(5, 1, 1 - x, c)
    fwd_xd = move(6, 1, 1, 1 - x, c, core_peer)
    fwd_xd.start()
    forward(1, 2)
    forward(1, 3)
    arrived(4, 1, x, 1 - c)
    arrived(6, 1, 1 - x, 1 - c)
    act[1] = jnp.dot(rows[1], wg[...], preferred_element_type=F32)
    for step in range(1, count):
        arrived_y(1, source_at(step))

    def up_step(p, carry):
        gate = act[p]
        up = jnp.dot(rows[p], wu[...], preferred_element_type=F32)
        start = pl.multiple_of(p * tokens, tokens)
        inner[pl.ds(start, tokens), :] = (gate / (1.0 + jnp.exp(-gate)) * up).astype(BF16)
        return carry

    lax.fori_loop(0, 2, up_step, 0)

    rounds = count * SUBS
    chunks2 = 2 * rounds
    base = 2 * lax.div(s, 2)

    def place_of(p):
        is_y = jnp.logical_or(
            jnp.logical_and(p > 0, lax.rem(p, 2) == 0), p == chunks2 - 1
        )
        last_one = p == chunks2 - 1
        r = jnp.where(
            last_one, rounds - 1,
            jnp.where(is_y, lax.div(p, 2) - 1, lax.div(p + 1, 2)),
        )
        r = jnp.maximum(r, 0)
        span = 2 * SUBS
        b = lax.rem(base + lax.div(r, span) * 2 + lax.rem(r, 2), count)
        sub = lax.rem(lax.div(r, 2), SUBS)
        which = jnp.where(is_y, 1 - g, g)
        return b, sub, which, is_y

    def down_rows(p):
        b, sub, which, _ = place_of(p)
        return b * depth + which * part_rows + sub * sub_rows

    def d2(k):
        return remote(dsend2.at[k], drecv2.at[k], d2s.at[k], d2r.at[k], core_peer)

    def x2(k):
        return remote(xsend2.at[k], xrecv2.at[k], x2s.at[k], x2r.at[k], x_peer)

    def z2(k):
        return remote(zsend2.at[k], zrecv2.at[k], z2s.at[k], z2r.at[k], pair)

    def down_step(p, carry):
        @pl.when(p < chunks2)
        def _():
            b, sub, _, is_y = place_of(p)
            start = pl.multiple_of(down_rows(p), sub_rows)
            spot = wd.at[pl.ds(start, sub_rows)]
            pid = 2 + sub
            z_in = remote(spot, spot, zs.at[pid, b], zr.at[pid, b], y_peer)
            y_both = remote(spot, spot, ys.at[pid, b], yr.at[pid, b], y_peer)

            @pl.when(jnp.logical_and(b != s, jnp.logical_not(is_y)))
            def _():
                z_in.wait_recv()
                y_both.start()

            @pl.when(jnp.logical_and(b != s, is_y))
            def _():
                y_both.wait_recv()

            part2[...] = lax.dot_general(
                inner[...], wd[pl.ds(start, sub_rows), :], NT, preferred_element_type=F32
            )
            ring = lax.rem(p, RING)
            for place in range(2):
                for role in range(2):
                    chip = x if role == 0 else 1 - x
                    send = pl.multiple_of(place * tokens + (2 * chip + 1 - c) * block, 8)
                    hold = pl.multiple_of(place * tokens + (2 * chip + c) * block, 8)
                    dsend2[p, 2 * place + role] = part2[pl.ds(send, block)].astype(BF16)
                    keep2[ring, 2 * place + role] = part2[pl.ds(hold, block)]
            d2(p).start()

        @pl.when(jnp.logical_and(p >= LAG_B, p < chunks2 + LAG_B))
        def _():
            k = p - LAG_B
            ring = lax.rem(k, RING)
            d2(k).wait_recv()
            for place in range(2):
                xsend2[k, place] = (
                    keep2[ring, 2 * place + 1] + drecv2[k, 2 * place + 1].astype(F32)
                ).astype(BF16)
            x2(k).start()
            for place in range(2):
                keep2[ring, 2 * place] = keep2[ring, 2 * place] + drecv2[
                    k, 2 * place
                ].astype(F32)

        @pl.when(jnp.logical_and(p >= LAG_C, p < chunks2 + LAG_C))
        def _():
            k = p - LAG_C
            ring = lax.rem(k, RING)
            x2(k).wait_recv()
            zsend2[k] = (keep2[ring, 2] + xrecv2[k, 1].astype(F32)).astype(BF16)
            z2(k).start()
            span = pl.ds(pl.multiple_of(down_rows(k), sub_rows), sub_rows)
            rsum[:, span] = rsum[:, span] + keep2[ring, 0] + xrecv2[k, 0].astype(F32)

        @pl.when(p >= LAG_D)
        def _():
            k = p - LAG_D
            z2(k).wait_recv()
            span = pl.ds(pl.multiple_of(down_rows(k), sub_rows), sub_rows)
            out_ref[:, span] = (rsum[:, span] + zrecv2[k].astype(F32)).astype(BF16)

        return carry

    lax.fori_loop(0, chunks2 + LAG_D, down_step, 0)

    for pid in range(2 + SUBS):
        for dest in range(count):
            @pl.when(dest != s)
            def _():
                z_copy(pid, dest).wait_send()
                y_copy(pid, dest, g).wait_send()

    @pl.when(s < last)
    def _():
        for copy in chain:
            copy.wait_send()

    for copy in (own_z, own_x, own_d, fwd_x, fwd_zx, fwd_zd, fwd_xd):
        copy.wait_send()
    for j in range(chunks1):
        d1(j).wait_send()
        x1(j).wait_send()

    def drain(k, carry):
        d2(k).wait_send()
        x2(k).wait_send()
        z2(k).wait_send()
        return carry

    lax.fori_loop(0, chunks2, drain, 0)


def fused(*args):
    query_a, _, _, _, _ = args[:5]
    resid, w_gate = args[10], args[13]
    count = lax.axis_size("sp")
    tokens = query_a.shape[0]
    heads = query_a.shape[1] // DKA
    depth, units = w_gate.shape
    half = units // 2
    block, width = resid.shape
    chunk1 = width // 4
    chunk2 = depth // 2 // SUBS
    chunks1, chunks2 = width // chunk1, width // chunk2
    group = 2 * heads
    state_rows = heads * (DKA + DKB)
    sizes = (count, tokens, heads, depth, half, block, chunk1, chunk2)
    args = list(args)
    args[12] = args[12].reshape(1, width)
    vmem = lambda *shape, kind=BF16: pltpu.VMEM(shape, kind)
    dma = pltpu.SemaphoreType.DMA
    pieces = (2 + SUBS, count)
    copies = [args[i] for i in (0, 1, 2, 3, 4, 5, 6, 7, 8, 9, 10, 11, 12)]
    scratch = [pltpu.VMEM(a.shape, a.dtype) for a in copies]
    scratch += [vmem(width, half), vmem(width, half), vmem(width, half)]
    scratch += [
        vmem(tokens, 2 * group, kind=F32),
        vmem(2 * group, tokens, kind=F32),
        vmem(state_rows, DV, kind=F32),
        vmem(state_rows, DV),
        vmem(state_rows, DV),
        vmem(2 * group, 128, kind=F32),
        vmem(2 * group, 128, kind=F32),
        vmem(group, tokens, DV, kind=F32),
        vmem(tokens, group * DV),
        vmem(tokens, chunk1, kind=F32),
        vmem(chunks1, 2, block, chunk1, kind=F32),
        vmem(chunks1, 2, block, chunk1),
        vmem(chunks1, 2, block, chunk1),
        vmem(chunks1, block, chunk1),
        vmem(chunks1, block, chunk1),
        vmem(block, width, kind=F32),
        vmem(2, tokens, width),
        vmem(2, tokens, half, kind=F32),
        vmem(2 * tokens, half),
        vmem(2 * tokens, chunk2, kind=F32),
        vmem(RING, 4, block, chunk2, kind=F32),
        vmem(chunks2, 4, block, chunk2),
        vmem(chunks2, 4, block, chunk2),
        vmem(chunks2, 2, block, chunk2),
        vmem(chunks2, 2, block, chunk2),
        vmem(chunks2, block, chunk2),
        vmem(chunks2, block, chunk2),
    ]
    scratch += [dma((16,)), dma(pieces), dma(pieces), dma(pieces), dma(pieces), dma((2,)), dma((2,))]
    scratch += [dma((chunks1,))] * 4 + [dma((7,))] * 2 + [dma((chunks2,))] * 6
    return pl.pallas_call(
        functools.partial(fused_body, sizes),
        out_shape=jax.ShapeDtypeStruct(resid.shape, BF16),
        in_specs=[pl.BlockSpec(memory_space=pl.ANY)] * len(args),
        out_specs=pl.BlockSpec(memory_space=pltpu.VMEM),
        scratch_shapes=scratch,
        compiler_params=pltpu.CompilerParams(
            collective_id=0, has_side_effects=True, vmem_limit_bytes=VMEM_BYTES
        ),
    )(*args)


def layer(*args):
    return local(*args)


def solution(mesh):
    few = mesh.shape["sp"] == 4 and mesh.shape["tp"] == 4
    return jax.shard_map(
        fused if few else layer,
        mesh=mesh,
        in_specs=(
            P(("grp", "sp"), "tp"),
            P(("grp", "sp"), "tp"),
            P(("grp", "sp"), "tp"),
            P(("grp", "sp"), "tp"),
            P(("grp", "sp"), "tp"),
            P(("grp", "sp"), "tp"),
            P(("grp", "sp"), "tp"),
            P(("grp", "sp"), "tp"),
            P(None, "tp", ("grp", "sp")),
            P(None, "tp", ("grp", "sp")),
            P(("grp", "sp", "tp"), None),
            P(None, None, "tp"),
            P(),
            P("sp", "tp"),
            P("sp", "tp"),
            P("sp", "tp"),
        ),
        out_specs=P(("grp", "sp", "tp"), None),
        check_vma=False,
    )
```

profile of v0, /device:TPU:24, one launch (start us, length us, event | category | flops | bytes accessed | tf_op | source)
XLA Modules:
  0.0 153.5 jit_solution(13095641921905633369)
XLA Ops:
  0.0 151.8 %shard_map.154 = bf16[96,2048]{1,0:T(8,128)(2,1)} custom-call(bf16[384,256]{1,0:T(8,128)(2,1)} %query_a.1, bf16[384,256]{1,0:T(8,128)(2,1)} %key_a.1, bf16[384,128]{1,0:T(8,128)(2,1)} %query_b.1, bf16[384,128]{1,0:T(8,128)(2,1)} %key_b.1, bf16[384,512]{1,0:T(8,128)(2,1)} %values_a.1, bf16[384,512]{1,0:T(8,128)(2,1)} %values_b.1, bf16[384,512]{1,0:T(8,128)(2,1)} %outgate_a.1, ...), custom_call_target="tpu_custom_call" | custom-call | tf_op jit(solution)/shard_map/pallas_call | solution.py:875
  151.8 1.8 %copy.18 = bf16[96,2048]{1,0:T(8,128)(2,1)} copy(bf16[96,2048]{1,0:T(8,128)(2,1)} %shard_map.154) | data formatting | bytes 786432
where the time goes:
time: 154 us
  Pallas kernels  152 us (99%)
  local copies, waits for them, and re-layouts  1.77 us (1%)
    pallas_call x1, Pallas kernels, fused(): pl.pallas_call(functools.partial(fused_body, sizes), out_shape=jax.ShapeD...  152 us

commit v1 on v0

--- a/solution.py
+++ b/solution.py
@@ -317,6 +317,24 @@
 SUBS = 2
 LAG_B, LAG_C, LAG_D, RING = 2, 5, 8, 8
 VMEM_BYTES = 60 * 2**20
+
+
+SENDS = (
+    (((0, 1),), ((1, 1), (2, 1), (3, 1)), ((0, 2), (1, 2), (0, 3), (1, 3)), ((2, 2), (3, 2), (2, 3), (3, 3)), ((4, 3), (4, 2), (4, 1), (5, 3), (5, 2), (5, 1))),
+    (((0, 0), (1, 0), (2, 0), (3, 0), (0, 2), (1, 2)), ((2, 2), (3, 2)), ((0, 3), (1, 3), (2, 3), (3, 3), (4, 3), (4, 2), (5, 3), (5, 2)), ((4, 0), (5, 0)), ()),
+    (((0, 0), (0, 1), (1, 0), (1, 1), (2, 0), (2, 1), (3, 0), (3, 1), (4, 0), (4, 1), (5, 0), (5, 1), (0, 3), (1, 3)), ((2, 3), (3, 3)), (), ((4, 3), (5, 3)), ()),
+    (((0, 0), (0, 1), (0, 2), (1, 0), (1, 1), (1, 2), (2, 0), (2, 1), (2, 2), (3, 0), (3, 1), (3, 2)), (), (), (), ((4, 0), (4, 1), (4, 2), (5, 0), (5, 1), (5, 2))),
+)
+FORWARDS = (
+    ((), ((0, 3),), ((0, 1), (0, 2), (1, 3), (1, 1)), ((2, 1), (2, 3), (3, 1), (1, 2)), ((3, 3), (2, 2)), (), ((3, 2), (4, 1)), (), ()),
+    (((0, 0), (0, 3)), (), ((1, 0), (2, 0), (1, 3), (3, 0), (0, 2)), ((2, 3),), ((3, 3),), ((1, 2),), ((2, 2),), (), ((3, 2),)),
+    (((0, 1), (1, 1), (0, 3)), (), ((2, 1), (1, 3), (0, 0), (1, 0)), ((2, 3), (3, 1), (3, 3)), ((2, 0), (3, 0)), (), (), (), ()),
+    (((0, 2), (1, 2)), (), ((2, 2), (0, 0), (1, 0), (3, 2)), ((0, 1),), ((2, 0), (3, 0), (1, 1), (2, 1)), ((3, 1),), ((4, 0),), (), ()),
+)
+ROUNDS = (
+    ((1, 0), (3, 0), (1, 1), (0, 0), (2, 0), (3, 1), (2, 1), (0, 1)),
+    ((3, 0), (0, 0), (2, 0), (0, 1), (3, 1), (2, 1), (1, 0), (1, 1)),
+)
 
 
 def scan_lanes(value, combine, neutral):
@@ -393,23 +411,21 @@
         (w_down.at[:, own_cols], wd.at[own_rows]),
     ]
     local = [pltpu.make_async_copy(a, b, lsem.at[i]) for i, (a, b) in enumerate(loads)]
-    for copy in local:
+    for copy in local[:8]:
         copy.start()
 
-    whole_of = (wg, wu) + (wd,) * SUBS
-    held_of = (w_gate, w_up) + (w_down,) * SUBS
+    whole_of = (wg,) * SUBS + (wu,) * SUBS + (wd,) * SUBS
+    held_of = (w_gate,) * SUBS + (w_up,) * SUBS + (w_down,) * SUBS
+    gates, ups, _ = (range(i * SUBS, (i + 1) * SUBS) for i in range(3))
 
     def piece_rows(pid, source, which):
-        if pid < 2:
-            return pl.ds(pl.multiple_of(source * depth + which * part_rows, part_rows), part_rows)
-        start = source * depth + which * part_rows + (pid - 2) * sub_rows
+        start = source * depth + which * part_rows + (pid % SUBS) * sub_rows
         return pl.ds(pl.multiple_of(start, sub_rows), sub_rows)
 
     def z_copy(pid, dest):
-        start = g * part_rows + (0 if pid < 2 else (pid - 2) * sub_rows)
-        size = part_rows if pid < 2 else sub_rows
+        start = g * part_rows + (pid % SUBS) * sub_rows
         src = held_of[pid].at[
-            pl.ds(pl.multiple_of(start, sub_rows), size), pl.ds((dest % 2) * half, half)
+            pl.ds(pl.multiple_of(start, sub_rows), sub_rows), pl.ds((dest % 2) * half, half)
         ]
         return remote(
             src, whole_of[pid].at[piece_rows(pid, s, g)],
@@ -424,42 +440,25 @@
         place = whole_of[pid].at[piece_rows(pid, source, g)]
         remote(place, place, zs.at[pid, source], zr.at[pid, source], y_peer).wait_recv()
 
-    def issue(pids, want):
-        for pid in pids:
-            for dest in list(range(count)):
-                @pl.when(jnp.logical_and(dest < s, want(dest)))
-                def _():
+    last = count - 1
+
+    def issue(point):
+        for place, plan in enumerate(SENDS):
+            @pl.when(s == place)
+            def _():
+                for pid, dest in plan[point]:
                     z_copy(pid, dest).start()
-            for dest in reversed(range(count)):
-                @pl.when(jnp.logical_and(dest > s, want(dest)))
-                def _():
-                    z_copy(pid, dest).start()
-
-    last = count - 1
-    at_end = jnp.logical_or(s == 0, s == last)
-
-    def far(dest):
-        return jnp.logical_or(jnp.logical_not(at_end), jnp.abs(dest - s) == last)
-
-    def near(dest):
-        return jnp.logical_not(far(dest))
-
-    def source_at(step):
-        up_room, down_room = last - s, s
-        small = jnp.minimum(up_room, down_room)
-        both = jnp.where(step % 2 == 1, s + (step + 1) // 2, s - step // 2)
-        beyond = jnp.where(up_room > down_room, s + step - small, s - step + small)
-        return jnp.where(step <= 2 * small, both, beyond)
-
-    def forward(pid, step):
-        source = source_at(step)
-        arrived_z(pid, source)
-        y_copy(pid, source, g).start()
+
+    def serve(point):
+        for place, plan in enumerate(FORWARDS):
+            @pl.when(s == place)
+            def _():
+                for pid, source in plan[point]:
+                    arrived_z(pid, source)
+                    y_copy(pid, source, g).start()
 
     pl.semaphore_wait(barrier, 3 + count - 1)
-    issue((0,), lambda dest: dest < s)
-    issue((1,), lambda dest: jnp.logical_and(dest < s, far(dest)))
-    issue((0,), lambda dest: dest > s)
+    issue(0)
 
     for i in range(2):
         local[i].wait()
@@ -499,36 +498,44 @@
         bstate[base_b + h * DKB : base_b + (h + 1) * DKB, :] = state[h * DKB : (h + 1) * DKB]
         state_of.append((base_b + h * DKB, DKB, heads + h))
 
+    after_peer = (g, jnp.minimum(s + 1, last), t)
     chain = [
-        remote(st_out, st_in, cs.at[0], cr.at[0], (g, jnp.minimum(s + 1, last), t)),
-        remote(stat_out, stat_in, cs.at[1], cr.at[1], (g, jnp.minimum(s + 1, last), t)),
+        remote(
+            st_out.at[pl.ds(start, size)], st_in.at[pl.ds(start, size)],
+            cs.at[h], cr.at[h], after_peer,
+        )
+        for start, size, h in state_of
     ]
-
-    def combine_and_send():
+    chain_stat = remote(stat_out, stat_in, cs.at[group], cr.at[group], after_peer)
+    wide = lambda row: jnp.concatenate([row] * (DV // 128), axis=1)
+
+    def combine_stat():
         before = stat_in[...]
         total = before + fsum
         after = jnp.maximum(total, bmax)
-        keep_old = jnp.exp(total - after)
-        keep_new = jnp.exp(jnp.broadcast_to(bmax, total.shape) - after)
         stat_out[...] = after
-        wide = lambda row: jnp.concatenate([row] * (DV // 128), axis=1)
-        for start, size, h in state_of:
-            old = wide(keep_old[h : h + 1, :])
-            new = wide(keep_new[h : h + 1, :])
-            st_out[start : start + size, :] = (
-                old * st_in[start : start + size, :].astype(F32)
-                + new * bstate[start : start + size, :]
-            ).astype(BF16)
-        for copy in chain:
-            copy.start()
+        chain_stat.start()
+        return jnp.exp(total - after), jnp.exp(jnp.broadcast_to(bmax, total.shape) - after)
+
+    def combine_head(i, keep_old, keep_new):
+        start, size, h = state_of[i]
+        st_out[start : start + size, :] = (
+            wide(keep_old[h : h + 1, :]) * st_in[start : start + size, :].astype(F32)
+            + wide(keep_new[h : h + 1, :]) * bstate[start : start + size, :]
+        ).astype(BF16)
+        chain[i].start()
 
     @pl.when(s == 0)
     def _():
         st_in[...] = jnp.zeros_like(st_in)
         stat_in[...] = jnp.full_like(stat_in, NEG)
-        combine_and_send()
-        issue((1,), lambda dest: jnp.logical_and(dest > s, far(dest)))
-
+        keeps = combine_stat()
+        for i in range(group):
+            combine_head(i, *keeps)
+        issue(1)
+
+    for copy in local[8:]:
+        copy.start()
     for i in range(6, 8):
         local[i].wait()
     causal = lax.broadcasted_iota(jnp.int32, (tokens, tokens), 0) >= lax.broadcasted_iota(
@@ -551,16 +558,22 @@
             weights, value_ref[:, at * DV : (at + 1) * DV], preferred_element_type=F32
         )
 
-    @pl.when(s > 0)
+    @pl.when(jnp.logical_and(s > 0, s < last))
     def _():
+        chain_stat.wait_recv()
+        keeps = combine_stat()
+        for i in range(group):
+            chain[i].wait_recv()
+            combine_head(i, *keeps)
+        issue(1)
+
+    @pl.when(s == last)
+    def _():
+        chain_stat.wait_recv()
         for copy in chain:
             copy.wait_recv()
 
-    @pl.when(jnp.logical_and(s > 0, s < last))
-    def _():
-        combine_and_send()
-        issue((1,), lambda dest: jnp.logical_and(dest > s, far(dest)))
-
+    serve(0)
     for i in range(8, 10):
         local[i].wait()
     for h in range(group):
@@ -580,7 +593,7 @@
         gated = numer * inv * jax.nn.sigmoid(gate_ref[:, at * DV : (at + 1) * DV].astype(F32))
         hidden[:, h * DV : (h + 1) * DV] = gated.astype(BF16)
 
-    forward(0, 1)
+    serve(1)
 
     for i in range(10, 13):
         local[i].wait()
@@ -620,7 +633,8 @@
         return carry
 
     lax.fori_loop(0, chunks1 + 1, attn_step, 0)
-    forward(0, 2)
+    issue(2)
+    serve(2)
     for j in range(chunks1):
         span = slice(j * chunk1, (j + 1) * chunk1)
         x1(j).wait_recv()
@@ -643,43 +657,47 @@
     own_z.start()
     own_x.start()
     own_d.start()
-    issue((1,), near)
-    issue(range(2, 2 + SUBS), lambda dest: dest != s)
+    issue(3)
 
     def arrived(kind, place, chip, core):
         move(kind, place, place, chip, core, core_peer).wait_recv()
 
-    forward(0, 3)
+    serve(3)
     arrived(1, 0, 1 - x, c)
     fwd_x = move(3, 0, 0, 1 - x, c, core_peer)
     fwd_x.start()
-    forward(1, 1)
+    serve(4)
     arrived(2, 1, x, c)
     fwd_zx = move(5, 1, 1, x, c, x_peer)
     fwd_zd = move(4, 1, 1, x, c, core_peer)
     fwd_zx.start()
     fwd_zd.start()
-
-    def arrived_y(pid, source):
-        y_copy(pid, source, 1 - g).wait_recv()
+    serve(5)
+
+    def take_y(pids):
+        for place in range(count):
+            @pl.when(place != s)
+            def _():
+                for pid in pids:
+                    y_copy(pid, place, 1 - g).wait_recv()
 
     for i in range(13, 16):
         local[i].wait()
-    for step in range(1, count):
-        arrived_y(0, source_at(step))
+    take_y(gates)
     arrived(0, 0, x, 1 - c)
     arrived(3, 0, 1 - x, 1 - c)
     act[0] = jnp.dot(rows[0], wg[...], preferred_element_type=F32)
+    serve(6)
     arrived(5, 1, 1 - x, c)
+    issue(4)
     fwd_xd = move(6, 1, 1, 1 - x, c, core_peer)
     fwd_xd.start()
-    forward(1, 2)
-    forward(1, 3)
+    serve(7)
     arrived(4, 1, x, 1 - c)
     arrived(6, 1, 1 - x, 1 - c)
     act[1] = jnp.dot(rows[1], wg[...], preferred_element_type=F32)
-    for step in range(1, count):
-        arrived_y(1, source_at(step))
+    serve(8)
+    take_y(ups)
 
     def up_step(p, carry):
         gate = act[p]
@@ -692,26 +710,42 @@
 
     rounds = count * SUBS
     chunks2 = 2 * rounds
-    base = 2 * lax.div(s, 2)
+
+    def look(table, k):
+        value = jnp.int32(table[0])
+        for i, entry in enumerate(table[1:], 1):
+            value = jnp.where(k == i, entry, value)
+        return value
+
+    low = s < count // 2
 
     def place_of(p):
         is_y = jnp.logical_or(
             jnp.logical_and(p > 0, lax.rem(p, 2) == 0), p == chunks2 - 1
         )
-        last_one = p == chunks2 - 1
         r = jnp.where(
-            last_one, rounds - 1,
+            p == chunks2 - 1, rounds - 1,
             jnp.where(is_y, lax.div(p, 2) - 1, lax.div(p + 1, 2)),
         )
         r = jnp.maximum(r, 0)
-        span = 2 * SUBS
-        b = lax.rem(base + lax.div(r, span) * 2 + lax.rem(r, 2), count)
-        sub = lax.rem(lax.div(r, 2), SUBS)
+        b, sub = (
+            jnp.where(low, *(look([pick[i] for pick in order], r) for order in ROUNDS))
+            for i in range(2)
+        )
         which = jnp.where(is_y, 1 - g, g)
-        return b, sub, which, is_y
+        return b, sub, which, is_y, r
+
+    def is_late(r):
+        value = jnp.bool_(False)
+        for place, plan in enumerate(FORWARDS):
+            done = {pair_ for point in plan for pair_ in point}
+            for k, (b, sub) in enumerate(ROUNDS[0 if place < count // 2 else 1]):
+                if b != place and (2 * SUBS + sub, b) not in done:
+                    value = jnp.logical_or(value, jnp.logical_and(s == place, r == k))
+        return value
 
     def down_rows(p):
-        b, sub, which, _ = place_of(p)
+        b, sub, which, _, _ = place_of(p)
         return b * depth + which * part_rows + sub * sub_rows
 
     def d2(k):
@@ -726,17 +760,19 @@
     def down_step(p, carry):
         @pl.when(p < chunks2)
         def _():
-            b, sub, _, is_y = place_of(p)
+            b, sub, _, is_y, r = place_of(p)
             start = pl.multiple_of(down_rows(p), sub_rows)
             spot = wd.at[pl.ds(start, sub_rows)]
-            pid = 2 + sub
+            pid = 2 * SUBS + sub
             z_in = remote(spot, spot, zs.at[pid, b], zr.at[pid, b], y_peer)
             y_both = remote(spot, spot, ys.at[pid, b], yr.at[pid, b], y_peer)
 
             @pl.when(jnp.logical_and(b != s, jnp.logical_not(is_y)))
             def _():
-                z_in.wait_recv()
-                y_both.start()
+                @pl.when(is_late(r))
+                def _():
+                    z_in.wait_recv()
+                    y_both.start()
 
             @pl.when(jnp.logical_and(b != s, is_y))
             def _():
@@ -791,7 +827,7 @@
 
     lax.fori_loop(0, chunks2 + LAG_D, down_step, 0)
 
-    for pid in range(2 + SUBS):
+    for pid in range(3 * SUBS):
         for dest in range(count):
             @pl.when(dest != s)
             def _():
@@ -800,6 +836,7 @@
 
     @pl.when(s < last)
     def _():
+        chain_stat.wait_send()
         for copy in chain:
             copy.wait_send()
 
@@ -837,7 +874,7 @@
     args[12] = args[12].reshape(1, width)
     vmem = lambda *shape, kind=BF16: pltpu.VMEM(shape, kind)
     dma = pltpu.SemaphoreType.DMA
-    pieces = (2 + SUBS, count)
+    pieces = (3 * SUBS, count)
     copies = [args[i] for i in (0, 1, 2, 3, 4, 5, 6, 7, 8, 9, 10, 11, 12)]
     scratch = [pltpu.VMEM(a.shape, a.dtype) for a in copies]
     scratch += [vmem(width, half), vmem(width, half), vmem(width, half)]
@@ -870,7 +907,7 @@
         vmem(chunks2, block, chunk2),
         vmem(chunks2, block, chunk2),
     ]
-    scratch += [dma((16,)), dma(pieces), dma(pieces), dma(pieces), dma(pieces), dma((2,)), dma((2,))]
+    scratch += [dma((16,)), dma(pieces), dma(pieces), dma(pieces), dma(pieces), dma((group + 1,)), dma((group + 1,))]
     scratch += [dma((chunks1,))] * 4 + [dma((7,))] * 2 + [dma((chunks2,))] * 6
     return pl.pallas_call(
         functools.partial(fused_body, sizes),

time: 154 us -> 129 us (0.84)
  Pallas kernels: 152 us -> 127 us
    pallas_call x1, Pallas kernels: 152 us -> 127 us  [fused(): pl.pallas_call(functools.partial(fused_body, sizes), out_shape=jax.ShapeD...]
where the time goes in v1:
time: 129 us
  Pallas kernels  127 us (98%)
  local copies, waits for them, and re-layouts  1.77 us (1%)
    pallas_call x1, Pallas kernels, fused(): pl.pallas_call(functools.partial(fused_body, sizes), out_shape=jax.ShapeD...  127 us

profile of v1, /device:TPU:24, one launch (start us, length us, event | category | flops | bytes accessed | tf_op | source)
XLA Modules:
  0.0 129.0 jit_solution(10233353496246184454)
XLA Ops:
  0.0 127.2 %shard_map.154 = bf16[96,2048]{1,0:T(8,128)(2,1)} custom-call(bf16[384,256]{1,0:T(8,128)(2,1)} %query_a.1, bf16[384,256]{1,0:T(8,128)(2,1)} %key_a.1, bf16[384,128]{1,0:T(8,128)(2,1)} %query_b.1, bf16[384,128]{1,0:T(8,128)(2,1)} %key_b.1, bf16[384,512]{1,0:T(8,128)(2,1)} %values_a.1, bf16[384,512]{1,0:T(8,128)(2,1)} %values_b.1, bf16[384,512]{1,0:T(8,128)(2,1)} %outgate_a.1, ...), custom_call_target="tpu_custom_call" | custom-call | tf_op jit(solution)/shard_map/pallas_call | solution.py:912
  127.2 1.8 %copy.18 = bf16[96,2048]{1,0:T(8,128)(2,1)} copy(bf16[96,2048]{1,0:T(8,128)(2,1)} %shard_map.154) | data formatting | bytes 786432

commit v2 on v1

--- a/solution.py
+++ b/solution.py
@@ -320,20 +320,26 @@
 
 
 SENDS = (
-    (((0, 1),), ((1, 1), (2, 1), (3, 1)), ((0, 2), (1, 2), (0, 3), (1, 3)), ((2, 2), (3, 2), (2, 3), (3, 3)), ((4, 3), (4, 2), (4, 1), (5, 3), (5, 2), (5, 1))),
-    (((0, 0), (1, 0), (2, 0), (3, 0), (0, 2), (1, 2)), ((2, 2), (3, 2)), ((0, 3), (1, 3), (2, 3), (3, 3), (4, 3), (4, 2), (5, 3), (5, 2)), ((4, 0), (5, 0)), ()),
-    (((0, 0), (0, 1), (1, 0), (1, 1), (2, 0), (2, 1), (3, 0), (3, 1), (4, 0), (4, 1), (5, 0), (5, 1), (0, 3), (1, 3)), ((2, 3), (3, 3)), (), ((4, 3), (5, 3)), ()),
-    (((0, 0), (0, 1), (0, 2), (1, 0), (1, 1), (1, 2), (2, 0), (2, 1), (2, 2), (3, 0), (3, 1), (3, 2)), (), (), (), ((4, 0), (4, 1), (4, 2), (5, 0), (5, 1), (5, 2))),
+    (((0, 1),), ((1, 1), (2, 1), (3, 1)), ((0, 2), (1, 2), (2, 2), (3, 2)), (), ((0, 3), (1, 3), (2, 3), (3, 3)), (), (), ((4, 1), (5, 1), (4, 3), (4, 2), (5, 3), (5, 2))),
+    (((0, 0), (1, 0), (2, 0), (3, 0), (0, 2), (1, 2)), ((2, 2), (3, 2)), ((4, 2), (5, 2)), (), (), ((0, 3), (1, 3), (2, 3), (3, 3), (4, 3), (5, 3)), ((4, 0), (5, 0)), ()),
+    (((0, 0), (0, 1), (1, 0), (1, 1), (2, 0), (2, 1), (3, 0), (3, 1), (4, 0), (4, 1), (5, 0), (5, 1), (0, 3), (1, 3), (4, 3)), ((2, 3), (3, 3), (5, 3)), (), (), (), (), (), ()),
+    (((0, 0), (0, 1), (0, 2), (1, 0), (1, 1), (1, 2), (2, 0), (2, 1), (2, 2), (3, 0), (3, 1), (3, 2)), (), (), (), (), ((4, 2), (5, 2), (4, 0), (4, 1), (5, 0), (5, 1)), (), ()),
 )
 FORWARDS = (
-    ((), ((0, 3),), ((0, 1), (0, 2), (1, 3), (1, 1)), ((2, 1), (2, 3), (3, 1), (1, 2)), ((3, 3), (2, 2)), (), ((3, 2), (4, 1)), (), ()),
+    ((), ((0, 3),), ((0, 1), (0, 2), (1, 3), (1, 1)), ((2, 1), (2, 3), (3, 1), (1, 2)), ((3, 3), (2, 2)), (), ((3, 2),), ((4, 1),), ((4, 3),)),
     (((0, 0), (0, 3)), (), ((1, 0), (2, 0), (1, 3), (3, 0), (0, 2)), ((2, 3),), ((3, 3),), ((1, 2),), ((2, 2),), (), ((3, 2),)),
-    (((0, 1), (1, 1), (0, 3)), (), ((2, 1), (1, 3), (0, 0), (1, 0)), ((2, 3), (3, 1), (3, 3)), ((2, 0), (3, 0)), (), (), (), ()),
-    (((0, 2), (1, 2)), (), ((2, 2), (0, 0), (1, 0), (3, 2)), ((0, 1),), ((2, 0), (3, 0), (1, 1), (2, 1)), ((3, 1),), ((4, 0),), (), ()),
+    (((0, 1), (1, 1), (0, 3)), (), ((2, 1), (1, 3)), ((0, 0), (1, 0), (2, 0), (2, 3), (3, 0), (3, 1), (4, 1)), ((3, 3),), (), ((4, 3), (5, 1), (5, 3)), (), ()),
+    (((0, 2), (1, 2), (4, 2)), ((2, 2),), (), ((3, 2), (5, 2)), (), ((0, 0), (1, 0), (2, 0), (3, 0), (0, 1), (1, 1)), (), ((2, 1),), ((3, 1),)),
+)
+LATE = (
+    ((), (), (), ((5, 1),), (), ((5, 3),), ((4, 2),), ((5, 2),)),
+    ((), ((4, 3), (4, 0)), (), (), ((5, 3), (5, 0)), (), ((4, 2),), ((5, 2),)),
+    ((), (), (), (), ((4, 0),), (), ((5, 0),), ()),
+    ((), (), (), (), ((4, 1), (4, 0)), (), ((5, 0),), ((5, 1),)),
 )
 ROUNDS = (
-    ((1, 0), (3, 0), (1, 1), (0, 0), (2, 0), (3, 1), (2, 1), (0, 1)),
-    ((3, 0), (0, 0), (2, 0), (0, 1), (3, 1), (2, 1), (1, 0), (1, 1)),
+    ((1, 0), (0, 0), (3, 0), (1, 1), (0, 1), (3, 1), (2, 0), (2, 1)),
+    ((2, 0), (3, 0), (2, 1), (3, 1), (0, 0), (1, 0), (0, 1), (1, 1)),
 )
 
 
@@ -449,13 +455,16 @@
                 for pid, dest in plan[point]:
                     z_copy(pid, dest).start()
 
+    def hand_on(pieces):
+        for pid, source in pieces:
+            arrived_z(pid, source)
+            y_copy(pid, source, g).start()
+
     def serve(point):
         for place, plan in enumerate(FORWARDS):
             @pl.when(s == place)
             def _():
-                for pid, source in plan[point]:
-                    arrived_z(pid, source)
-                    y_copy(pid, source, g).start()
+                hand_on(plan[point])
 
     pl.semaphore_wait(barrier, 3 + count - 1)
     issue(0)
@@ -663,6 +672,7 @@
         move(kind, place, place, chip, core, core_peer).wait_recv()
 
     serve(3)
+    issue(4)
     arrived(1, 0, 1 - x, c)
     fwd_x = move(3, 0, 0, 1 - x, c, core_peer)
     fwd_x.start()
@@ -672,6 +682,7 @@
     fwd_zd = move(4, 1, 1, x, c, core_peer)
     fwd_zx.start()
     fwd_zd.start()
+    issue(5)
     serve(5)
 
     def take_y(pids):
@@ -689,7 +700,7 @@
     act[0] = jnp.dot(rows[0], wg[...], preferred_element_type=F32)
     serve(6)
     arrived(5, 1, 1 - x, c)
-    issue(4)
+    issue(6)
     fwd_xd = move(6, 1, 1, 1 - x, c, core_peer)
     fwd_xd.start()
     serve(7)
@@ -707,6 +718,7 @@
         return carry
 
     lax.fori_loop(0, 2, up_step, 0)
+    issue(7)
 
     rounds = count * SUBS
     chunks2 = 2 * rounds
@@ -734,15 +746,6 @@
         )
         which = jnp.where(is_y, 1 - g, g)
         return b, sub, which, is_y, r
-
-    def is_late(r):
-        value = jnp.bool_(False)
-        for place, plan in enumerate(FORWARDS):
-            done = {pair_ for point in plan for pair_ in point}
-            for k, (b, sub) in enumerate(ROUNDS[0 if place < count // 2 else 1]):
-                if b != place and (2 * SUBS + sub, b) not in done:
-                    value = jnp.logical_or(value, jnp.logical_and(s == place, r == k))
-        return value
 
     def down_rows(p):
         b, sub, which, _, _ = place_of(p)
@@ -764,15 +767,16 @@
             start = pl.multiple_of(down_rows(p), sub_rows)
             spot = wd.at[pl.ds(start, sub_rows)]
             pid = 2 * SUBS + sub
-            z_in = remote(spot, spot, zs.at[pid, b], zr.at[pid, b], y_peer)
             y_both = remote(spot, spot, ys.at[pid, b], yr.at[pid, b], y_peer)
 
-            @pl.when(jnp.logical_and(b != s, jnp.logical_not(is_y)))
-            def _():
-                @pl.when(is_late(r))
-                def _():
-                    z_in.wait_recv()
-                    y_both.start()
+            for place, plan in enumerate(LATE):
+                for k, pieces in enumerate(plan):
+                    if pieces:
+                        now = jnp.logical_and(s == place, r == k)
+
+                        @pl.when(jnp.logical_and(now, jnp.logical_not(is_y)))
+                        def _():
+                            hand_on(pieces)
 
             @pl.when(jnp.logical_and(b != s, is_y))
             def _():

time: 129 us -> 123 us (0.953); the launches traced: 129 us -> 121 us
  Pallas kernels: 127 us -> 119 us
    pallas_call x1, Pallas kernels: 127 us -> 119 us  [fused(): pl.pallas_call(functools.partial(fused_body, sizes), out_shape=jax.ShapeD...]
where the time goes in v2:
time: 123 us; the launch traced here: 121 us
  Pallas kernels  119 us (97%)
  local copies, waits for them, and re-layouts  1.77 us (1%)
    pallas_call x1, Pallas kernels, fused(): pl.pallas_call(functools.partial(fused_body, sizes), out_shape=jax.ShapeD...  119 us

profile of v2, /device:TPU:24, one launch (start us, length us, event | category | flops | bytes accessed | tf_op | source)
XLA Modules:
  0.0 121.0 jit_solution(7384919649177652884)
XLA Ops:
  0.0 119.2 %shard_map.154 = bf16[96,2048]{1,0:T(8,128)(2,1)} custom-call(bf16[384,256]{1,0:T(8,128)(2,1)} %query_a.1, bf16[384,256]{1,0:T(8,128)(2,1)} %key_a.1, bf16[384,128]{1,0:T(8,128)(2,1)} %query_b.1, bf16[384,128]{1,0:T(8,128)(2,1)} %key_b.1, bf16[384,512]{1,0:T(8,128)(2,1)} %values_a.1, bf16[384,512]{1,0:T(8,128)(2,1)} %values_b.1, bf16[384,512]{1,0:T(8,128)(2,1)} %outgate_a.1, ...), custom_call_target="tpu_custom_call" | custom-call | tf_op jit(solution)/shard_map/pallas_call | solution.py:916
  119.2 1.8 %copy.18 = bf16[96,2048]{1,0:T(8,128)(2,1)} copy(bf16[96,2048]{1,0:T(8,128)(2,1)} %shard_map.154) | data formatting | bytes 786432

commit v3 on v2

--- a/solution.py
+++ b/solution.py
@@ -315,7 +315,7 @@
 F32 = jnp.float32
 BF16 = jnp.bfloat16
 SUBS = 2
-LAG_B, LAG_C, LAG_D, RING = 2, 5, 8, 8
+LAG_B, LAG_C, RING = 2, 5, 8
 VMEM_BYTES = 60 * 2**20
 
 
@@ -326,16 +326,16 @@
     (((0, 0), (0, 1), (0, 2), (1, 0), (1, 1), (1, 2), (2, 0), (2, 1), (2, 2), (3, 0), (3, 1), (3, 2)), (), (), (), (), ((4, 2), (5, 2), (4, 0), (4, 1), (5, 0), (5, 1)), (), ()),
 )
 FORWARDS = (
-    ((), ((0, 3),), ((0, 1), (0, 2), (1, 3), (1, 1)), ((2, 1), (2, 3), (3, 1), (1, 2)), ((3, 3), (2, 2)), (), ((3, 2),), ((4, 1),), ((4, 3),)),
+    ((), ((0, 3),), ((0, 1), (0, 2), (1, 3), (1, 1)), ((2, 1), (2, 3), (3, 1), (1, 2)), ((3, 3), (2, 2)), (), ((3, 2),), (), ()),
     (((0, 0), (0, 3)), (), ((1, 0), (2, 0), (1, 3), (3, 0), (0, 2)), ((2, 3),), ((3, 3),), ((1, 2),), ((2, 2),), (), ((3, 2),)),
     (((0, 1), (1, 1), (0, 3)), (), ((2, 1), (1, 3)), ((0, 0), (1, 0), (2, 0), (2, 3), (3, 0), (3, 1), (4, 1)), ((3, 3),), (), ((4, 3), (5, 1), (5, 3)), (), ()),
-    (((0, 2), (1, 2), (4, 2)), ((2, 2),), (), ((3, 2), (5, 2)), (), ((0, 0), (1, 0), (2, 0), (3, 0), (0, 1), (1, 1)), (), ((2, 1),), ((3, 1),)),
+    (((0, 2), (1, 2), (4, 2)), ((2, 2),), (), ((3, 2), (5, 2)), (), ((0, 0), (1, 0), (2, 0), (3, 0), (0, 1), (1, 1), (2, 1)), (), (), ((3, 1),)),
 )
 LATE = (
-    ((), (), (), ((5, 1),), (), ((5, 3),), ((4, 2),), ((5, 2),)),
-    ((), ((4, 3), (4, 0)), (), (), ((5, 3), (5, 0)), (), ((4, 2),), ((5, 2),)),
+    (((4, 1), (4, 3)), ((5, 1),), (), ((5, 3),), (), (), ((4, 2),), ((5, 2),)),
+    ((), ((4, 3), (4, 0)), (), ((5, 3), (5, 0)), (), (), ((4, 2),), ((5, 2),)),
     ((), (), (), (), ((4, 0),), (), ((5, 0),), ()),
-    ((), (), (), (), ((4, 1), (4, 0)), (), ((5, 0),), ((5, 1),)),
+    (((4, 0),), (), ((5, 0),), (), ((4, 1),), (), ((5, 1),), ()),
 )
 ROUNDS = (
     ((1, 0), (0, 0), (3, 0), (1, 1), (0, 1), (3, 1), (2, 0), (2, 1)),
@@ -760,6 +760,8 @@
     def z2(k):
         return remote(zsend2.at[k], zrecv2.at[k], z2s.at[k], z2r.at[k], pair)
 
+    lag_d = chunks2
+
     def down_step(p, carry):
         @pl.when(p < chunks2)
         def _():
@@ -820,16 +822,16 @@
             span = pl.ds(pl.multiple_of(down_rows(k), sub_rows), sub_rows)
             rsum[:, span] = rsum[:, span] + keep2[ring, 0] + xrecv2[k, 0].astype(F32)
 
-        @pl.when(p >= LAG_D)
+        @pl.when(p >= lag_d)
         def _():
-            k = p - LAG_D
+            k = p - lag_d
             z2(k).wait_recv()
             span = pl.ds(pl.multiple_of(down_rows(k), sub_rows), sub_rows)
             out_ref[:, span] = (rsum[:, span] + zrecv2[k].astype(F32)).astype(BF16)
 
         return carry
 
-    lax.fori_loop(0, chunks2 + LAG_D, down_step, 0)
+    lax.fori_loop(0, chunks2 + lag_d, down_step, 0)
 
     for pid in range(3 * SUBS):
         for dest in range(count):

time: 123 us -> 116 us (0.943)
  Pallas kernels: 119 us -> 112 us
    pallas_call x1, Pallas kernels: 119 us -> 112 us  [fused(): pl.pallas_call(functools.partial(fused_body, sizes), out_shape=jax.ShapeD...]
where the time goes in v3:
time: 116 us; the launch traced here: 113 us
  Pallas kernels  112 us (97%)
  local copies, waits for them, and re-layouts  1.77 us (2%)
    pallas_call x1, Pallas kernels, fused(): pl.pallas_call(functools.partial(fused_body, sizes), out_shape=jax.ShapeD...  112 us

profile of v3, /device:TPU:24, one launch (start us, length us, event | category | flops | bytes accessed | tf_op | source)
XLA Modules:
  0.0 113.3 jit_solution(9920718987279191754)
XLA Ops:
  0.0 111.6 %shard_map.154 = bf16[96,2048]{1,0:T(8,128)(2,1)} custom-call(bf16[384,256]{1,0:T(8,128)(2,1)} %query_a.1, bf16[384,256]{1,0:T(8,128)(2,1)} %key_a.1, bf16[384,128]{1,0:T(8,128)(2,1)} %query_b.1, bf16[384,128]{1,0:T(8,128)(2,1)} %key_b.1, bf16[384,512]{1,0:T(8,128)(2,1)} %values_a.1, bf16[384,512]{1,0:T(8,128)(2,1)} %values_b.1, bf16[384,512]{1,0:T(8,128)(2,1)} %outgate_a.1, ...), custom_call_target="tpu_custom_call" | custom-call | tf_op jit(solution)/shard_map/pallas_call | solution.py:918
  111.6 1.8 %copy.18 = bf16[96,2048]{1,0:T(8,128)(2,1)} copy(bf16[96,2048]{1,0:T(8,128)(2,1)} %shard_map.154) | data formatting | bytes 786432
